TPU v7x, 128 devices: a whole 4x4x4 slice. The times are simulated.
128 devices in a mesh: sp: 32 (over y, x, core), tp: 4 (over z).
Axes of the slice: x: 4, y: 4, z: 4, core: 2. Of those that a mesh axis runs over, the one named last changes fastest.
Arguments:
- sequence: bfloat16 [4, 1024, 1024], P(None, 'sp', 'tp'), may hold values from -6 to 6
- norm_gain: float32 [3, 1024], replicated, may hold values from 0.1 to 1.9
- weight_value: bfloat16 [3, 1024, 512], P(None, 'sp', 'tp'), may hold values from -0.1875 to 0.1875
- weight_outer: bfloat16 [3, 1024, 512], P(None, 'sp', 'tp'), may hold values from -0.1875 to 0.1875
- weight_inner: bfloat16 [3, 1024, 512], P(None, 'sp', 'tp'), may hold values from -0.1875 to 0.1875
- conv_taps: float32 [3, 3, 512], P(None, None, 'tp'), may hold values from -3 to 3
- weight_out: bfloat16 [3, 512, 1024], P(None, 'tp', 'sp'), may hold values from -0.25 to 0.25
Outputs:
- mixed: bfloat16 [4, 1024, 1024], P(None, 'sp', 'tp')
All inputs are finite; a program needn't handle non-finite values.
Results may differ from a plain program's by a relative error of at most 0.03.
Values may be sent and summed in bfloat16 or wider, within the bound.
A program may use at most 64 MiB of HBM per device.

v0:
```python
import jax
import jax.numpy as jnp
from jax import lax
from jax.sharding import PartitionSpec as P

LAYERS = 3


def folded(array, axis, dim, update, carry):
    whole = jax.tree.map(lambda part: lax.all_gather(part, axis, axis=dim, tiled=True), array)
    return update(carry, whole, jnp.int32(0))


def from_behind(value, axis, steps):
    count = lax.axis_size(axis)
    first, last = max(0, -steps), min(count, count - steps)
    return lax.ppermute(value, axis, [(source, source + steps) for source in range(first, last)])


def over_all(slab, axis, dim, apply):
    everything = lax.all_gather(slab, axis, axis=dim, tiled=True)
    return apply(everything, jnp.int32(0))


def rms_rows(values, gain_row):
    wide = values.astype(jnp.float32)
    scaled = wide * lax.rsqrt(jnp.mean(wide * wide, axis=-1, keepdims=True) + 1e-06)
    return (scaled * gain_row).astype(jnp.bfloat16)


def body(sequence, norm_gain, weight_value, weight_outer, weight_inner, conv_taps, weight_out):
    current = sequence
    seq_count = sequence.shape[0]
    local_len = sequence.shape[1]
    channels = weight_value.shape[2]
    depth = conv_taps.shape[1]
    for layer_index in range(LAYERS):
        whole = lax.all_gather(current, "tp", axis=2, tiled=True)
        normed = rms_rows(whole, norm_gain[layer_index]).reshape(
            seq_count * local_len, whole.shape[2]
        )
        empty = jnp.zeros((normed.shape[0], channels), jnp.float32)

        def add_rows(running, weight_rows, offset):
            columns = lax.dynamic_slice_in_dim(normed, offset, weight_rows.shape[0], 1)
            return running + jnp.dot(columns, weight_rows, preferred_element_type=jnp.float32)

        sum_value = folded(weight_value[layer_index], "sp", 0, add_rows, empty)
        sum_outer = folded(weight_outer[layer_index], "sp", 0, add_rows, empty)
        sum_inner = folded(weight_inner[layer_index], "sp", 0, add_rows, empty)
        proj_value = sum_value.astype(jnp.bfloat16)
        proj_outer = sum_outer.astype(jnp.bfloat16)
        proj_inner = sum_inner.astype(jnp.bfloat16)
        product = (proj_inner.astype(jnp.float32) * proj_value.astype(jnp.float32)).reshape(
            seq_count, local_len, channels
        )
        last_rows = product[:, local_len - (depth - 1) :, :]
        before = from_behind(last_rows, "sp", 1)
        padded = jnp.concatenate([before, product], axis=1)
        filtered = conv_taps[layer_index, 0] * padded[:, 0:local_len]
        for offset in range(1, depth):
            filtered = (
                filtered + conv_taps[layer_index, offset] * padded[:, offset : offset + local_len]
            )
        gated = (
            proj_outer.astype(jnp.float32).reshape(seq_count, local_len, channels) * filtered
        ).astype(jnp.bfloat16)
        gated_rows = gated.reshape(seq_count * local_len, channels)

        def project_columns(weight_cols, offset):
            return jnp.dot(gated_rows, weight_cols, preferred_element_type=jnp.float32)

        terms = over_all(weight_out[layer_index], "sp", 1, project_columns)
        shares = lax.psum_scatter(
            terms.astype(jnp.bfloat16), "tp", scatter_dimension=1, tiled=True
        ).astype(jnp.float32)
        shares = shares.reshape(seq_count, local_len, shares.shape[1])
        current = (current.astype(jnp.float32) + shares).astype(jnp.bfloat16)
    return current


def solution(mesh):
    return jax.shard_map(
        body,
        mesh=mesh,
        in_specs=(
            P(None, "sp", "tp"),
            P(),
            P(None, "sp", "tp"),
            P(None, "sp", "tp"),
            P(None, "sp", "tp"),
            P(None, None, "tp"),
            P(None, "tp", "sp"),
        ),
        out_specs=P(None, "sp", "tp"),
        check_vma=False,
    )
```

profile of v0, /device:TPU:1, one launch (start us, length us, event | category | flops | bytes accessed | tf_op | source)
XLA Modules:
  0.0 376.9 jit_solution(10216382479463195660)
XLA Ops:
  6.5 0.8 fusion.58
  7.4 12.5 %all_gather.45 = bf16[4,32,1024]{2,1,0:T(8,128)(2,1)S(1)} all-gather(bf16[4,32,256]{2,1,0:T(8,128)(2,1)} %param.7), channel_id=1, replica_groups=mesh['sp'=32,'tp'=4] {'tp'}, dimensions={2}, use_global_device_ids=true | all-gather | bytes 327680 | tf_op jit(solution)/shard_map/all_gather | solution.py:38
  20.1 0.6 copy-done.1
  20.7 27.6 %all-gather.1 = bf16[1,1024,128]{2,1,0:T(8,128)(2,1)S(1)} all-gather(bf16[1,32,128]{2,1,0:T(8,128)(2,1)S(1)} %get-tuple-element.15), channel_id=3, replica_groups=mesh['sp'=32,'tp'=4] {'sp'}, dimensions={1}, use_global_device_ids=true | all-gather | bytes 270336 | tf_op jit(solution)/shard_map/all_gather | solution.py:10
  48.2 24.0 %all-gather.2 = bf16[1,1024,128]{2,1,0:T(8,128)(2,1)S(1)} all-gather(bf16[1,32,128]{2,1,0:T(8,128)(2,1)S(1)} %get-tuple-element.12), channel_id=4, replica_groups=mesh['sp'=32,'tp'=4] {'sp'}, dimensions={1}, use_global_device_ids=true | all-gather | bytes 270336 | tf_op jit(solution)/shard_map/all_gather | solution.py:10
  72.9 1.9 collective-permute-start
  74.8 22.8 %all-gather = bf16[1,1024,128]{2,1,0:T(8,128)(2,1)S(1)} all-gather(bf16[1,32,128]{2,1,0:T(8,128)(2,1)S(1)} %get-tuple-element.9), channel_id=2, replica_groups=mesh['sp'=32,'tp'=4] {'sp'}, dimensions={1}, use_global_device_ids=true | all-gather | bytes 270336 | tf_op jit(solution)/shard_map/all_gather | solution.py:10
  97.8 0.5 copy-done.5
  98.4 24.0 %all-gather.3 = bf16[1,128,1024]{1,2,0:T(8,128)(2,1)S(1)} all-gather(bf16[1,128,32]{1,2,0:T(8,128)(2,1)S(1)} %get-tuple-element.6), channel_id=5, replica_groups=mesh['sp'=32,'tp'=4] {'sp'}, dimensions={2}, use_global_device_ids=true | all-gather | bytes 270336 | tf_op jit(solution)/shard_map/all_gather | solution.py:21
  122.4 0.9 convolution_convert_fusion.2
  123.4 22.4 %all-gather.5 = bf16[1,1024,128]{2,1,0:T(8,128)(2,1)S(1)} all-gather(bf16[1,32,128]{2,1,0:T(8,128)(2,1)S(1)} %get-tuple-element.16), channel_id=7, replica_groups=mesh['sp'=32,'tp'=4] {'sp'}, dimensions={1}, use_global_device_ids=true | all-gather | bytes 270336 | tf_op jit(solution)/shard_map/all_gather | solution.py:10
  145.9 24.0 %all-gather.6 = bf16[1,1024,128]{2,1,0:T(8,128)(2,1)S(1)} all-gather(bf16[1,32,128]{2,1,0:T(8,128)(2,1)S(1)} %get-tuple-element.13), channel_id=8, replica_groups=mesh['sp'=32,'tp'=4] {'sp'}, dimensions={1}, use_global_device_ids=true | all-gather | bytes 270336 | tf_op jit(solution)/shard_map/all_gather | solution.py:10
  169.9 22.6 %all-gather.4 = bf16[1,1024,128]{2,1,0:T(8,128)(2,1)S(1)} all-gather(bf16[1,32,128]{2,1,0:T(8,128)(2,1)S(1)} %get-tuple-element.10), channel_id=6, replica_groups=mesh['sp'=32,'tp'=4] {'sp'}, dimensions={1}, use_global_device_ids=true | all-gather | bytes 270336 | tf_op jit(solution)/shard_map/all_gather | solution.py:10
  192.5 24.2 %all-gather.7 = bf16[1,128,1024]{1,2,0:T(8,128)(2,1)S(1)} all-gather(bf16[1,128,32]{1,2,0:T(8,128)(2,1)S(1)} %get-tuple-element.7), channel_id=9, replica_groups=mesh['sp'=32,'tp'=4] {'sp'}, dimensions={2}, use_global_device_ids=true | all-gather | bytes 270336 | tf_op jit(solution)/shard_map/all_gather | solution.py:21
  216.7 0.9 fusion.32
  217.5 10.0 %all_gather.50 = bf16[4,32,1024]{2,1,0:T(8,128)(2,1)S(1)} all-gather(bf16[4,32,256]{2,1,0:T(8,128)(2,1)S(1)} %fusion.32), channel_id=1, replica_groups=mesh['sp'=32,'tp'=4] {'tp'}, dimensions={2}, use_global_device_ids=true | all-gather | bytes 327680 | tf_op jit(solution)/shard_map/all_gather | solution.py:38
  228.3 3.8 %collective-permute-start.1 = (f32[4,2,128]{2,1,0:T(2,128)S(1)}, f32[4,2,128]{2,1,0:T(2,128)S(1)}, u32[]{:S(2)}, u32[]{:S(2)}) collective-permute-start(f32[4,2,128]{2,1,0:T(2,128)S(1)} %slice.135), channel_id=1, source_target_pairs={{0,4},{4,8},{8,12},{12,16},{16,20},{20,24},{24,28},{28,32},{32,36}... | collective-permute-start | bytes 12296 | tf_op jit(solution)/shard_map/ppermute | solution.py:17
  232.2 0.2 convolution_convert_fusion.8
  232.4 0.5 collective-permute-done.1
  232.9 0.9 convolution_convert_fusion.1
  233.9 27.1 %all-gather.9 = bf16[1,1024,128]{2,1,0:T(8,128)(2,1)S(1)} all-gather(bf16[1,32,128]{2,1,0:T(8,128)(2,1)S(1)} %get-tuple-element.14), channel_id=11, replica_groups=mesh['sp'=32,'tp'=4] {'sp'}, dimensions={1}, use_global_device_ids=true | all-gather | bytes 270336 | tf_op jit(solution)/shard_map/all_gather | solution.py:10
  261.0 22.8 %all-gather.10 = bf16[1,1024,128]{2,1,0:T(8,128)(2,1)S(1)} all-gather(bf16[1,32,128]{2,1,0:T(8,128)(2,1)S(1)} %get-tuple-element.11), channel_id=12, replica_groups=mesh['sp'=32,'tp'=4] {'sp'}, dimensions={1}, use_global_device_ids=true | all-gather | bytes 270336 | tf_op jit(solution)/shard_map/all_gather | solution.py:10
  283.8 23.6 %all-gather.8 = bf16[1,1024,128]{2,1,0:T(8,128)(2,1)S(1)} all-gather(bf16[1,32,128]{2,1,0:T(8,128)(2,1)S(1)} %get-tuple-element.8), channel_id=10, replica_groups=mesh['sp'=32,'tp'=4] {'sp'}, dimensions={1}, use_global_device_ids=true | all-gather | bytes 270336 | tf_op jit(solution)/shard_map/all_gather | solution.py:10
  307.5 22.8 %all-gather.11 = bf16[1,128,1024]{1,2,0:T(8,128)(2,1)S(1)} all-gather(bf16[1,128,32]{1,2,0:T(8,128)(2,1)S(1)} %get-tuple-element.5), channel_id=13, replica_groups=mesh['sp'=32,'tp'=4] {'sp'}, dimensions={2}, use_global_device_ids=true | all-gather | bytes 270336 | tf_op jit(solution)/shard_map/all_gather | solution.py:21
  330.3 0.9 fusion.31
  331.2 10.1 %all_gather.55 = bf16[4,32,1024]{2,1,0:T(8,128)(2,1)S(1)} all-gather(bf16[4,32,256]{2,1,0:T(8,128)(2,1)S(1)} %fusion.31), channel_id=1, replica_groups=mesh['sp'=32,'tp'=4] {'tp'}, dimensions={2}, use_global_device_ids=true | all-gather | bytes 327680 | tf_op jit(solution)/shard_map/all_gather | solution.py:38
  342.0 4.7 %collective-permute-start.2 = (f32[4,2,128]{2,1,0:T(2,128)S(1)}, f32[4,2,128]{2,1,0:T(2,128)S(1)}, u32[]{:S(2)}, u32[]{:S(2)}) collective-permute-start(f32[4,2,128]{2,1,0:T(2,128)S(1)} %slice.138), channel_id=1, source_target_pairs={{0,4},{4,8},{8,12},{12,16},{16,20},{20,24},{24,28},{28,32},{32,36}... | collective-permute-start | bytes 12296 | tf_op jit(solution)/shard_map/ppermute | solution.py:17
  346.7 0.2 convolution_convert_fusion.5
  346.9 0.5 collective-permute-done.2
  347.4 0.9 convolution_convert_fusion
  348.4 20.5 %reduce-scatter.8.cloned.1.call-done = bf16[128,256]{1,0:T(8,128)(2,1)} async-done(((bf16[128,1024]{1,0:T(8,128)(2,1)}), bf16[128,256]{1,0:T(8,128)(2,1)}) %reduce-scatter.8.cloned.1.call-update) | async-done | bytes 65552 | tf_op jit(solution)/shard_map/reduce_scatter | solution.py:74
  368.9 1.5 fusion.30
  (46 shorter events, 2.7 us)
Async XLA Ops:
  6.5 210.1 %reduce-scatter.4.cloned.1.call-start = ((), (), s32[]{:S(2)}) async-start(), calls=%async_computation.3 | async-start | bytes 327680 | tf_op jit(solution)/shard_map/reduce_scatter | solution.py:74
  19.9 0.7 copy-start.1
  20.7 27.6 %copy-start.2 = (bf16[3,32,128]{2,1,0:T(8,128)(2,1)S(1)}, bf16[3,32,128]{2,1,0:T(8,128)(2,1)}, u32[]{:S(2)}) copy-start(bf16[3,32,128]{2,1,0:T(8,128)(2,1)} %param.9) | copy-start | bytes 73732
  72.6 2.2 copy-start.3
  72.9 49.5 %collective-permute-start = (f32[4,2,128]{2,1,0:T(2,128)S(1)}, f32[4,2,128]{2,1,0:T(2,128)S(1)}, u32[]{:S(2)}, u32[]{:S(2)}) collective-permute-start(f32[4,2,128]{2,1,0:T(2,128)S(1)} %slice.132), channel_id=1, source_target_pairs={{0,4},{4,8},{8,12},{12,16},{16,20},{20,24},{24,28},{28,32},{32,36}... | collective-permute-start | bytes 12296 | tf_op jit(solution)/shard_map/ppermute | solution.py:17
  97.6 0.7 copy-start.5
  97.6 0.8 copy-start.4
  123.4 206.9 %reduce-scatter.6.cloned.1.call-start = ((), (), s32[]{:S(2)}) async-start(), calls=%async_computation.4 | async-start | bytes 327680 | tf_op jit(solution)/shard_map/reduce_scatter | solution.py:74
  192.5 24.2 %copy-start = (bf16[4,32,256]{2,1,0:T(8,128)(2,1)S(1)}, bf16[4,32,256]{2,1,0:T(8,128)(2,1)}, u32[]{:S(2)}) copy-start(bf16[4,32,256]{2,1,0:T(8,128)(2,1)} %param.7) | copy-start | bytes 196612
  228.3 4.6 %collective-permute-start.1 = (f32[4,2,128]{2,1,0:T(2,128)S(1)}, f32[4,2,128]{2,1,0:T(2,128)S(1)}, u32[]{:S(2)}, u32[]{:S(2)}) collective-permute-start(f32[4,2,128]{2,1,0:T(2,128)S(1)} %slice.135), channel_id=1, source_target_pairs={{0,4},{4,8},{8,12},{12,16},{16,20},{20,24},{24,28},{28,32},{32,36}... | collective-permute-start | bytes 12296 | tf_op jit(solution)/shard_map/ppermute | solution.py:17
  233.9 135.0 %reduce-scatter.8.cloned.1.call-start = ((), (), s32[]{:S(2)}) async-start(), calls=%async_computation.5 | async-start | bytes 327680 | tf_op jit(solution)/shard_map/reduce_scatter | solution.py:74
  342.0 5.4 %collective-permute-start.2 = (f32[4,2,128]{2,1,0:T(2,128)S(1)}, f32[4,2,128]{2,1,0:T(2,128)S(1)}, u32[]{:S(2)}, u32[]{:S(2)}) collective-permute-start(f32[4,2,128]{2,1,0:T(2,128)S(1)} %slice.138), channel_id=1, source_target_pairs={{0,4},{4,8},{8,12},{12,16},{16,20},{20,24},{24,28},{28,32},{32,36}... | collective-permute-start | bytes 12296 | tf_op jit(solution)/shard_map/ppermute | solution.py:17
Sparse Core Ops, SparseCore 0:
  123.5 17.0 reduce-scatter.3
  234.0 20.4 reduce-scatter.5
  348.5 20.3 reduce-scatter.7
where the time goes:
time: 379 us; the launch traced here: 377 us
  blocking collectives  321 us (85%)
  waiting for transfers between devices  21.6 us (6%)
  between operations  13.4 us (4%)
  starting transfers between devices  10.5 us (3%)
  matrix products  4.77 us (1%)
  other arithmetic  4.12 us (1%)
    all_gather x9, blocking collectives, folded(): lax.all_gather(part, axis, axis=dim, tiled=True)  217 us
    all_gather x3, blocking collectives, over_all(): everything = lax.all_gather(slab, axis, axis=dim, tiled=True)  71 us
    all_gather x3, blocking collectives, body(): whole = lax.all_gather(current, 'tp', axis=2, tiled=True)  32.6 us
    reduce_scatter x3, waiting for transfers between devices, body(): lax.psum_scatter(terms.astype(jnp.bfloat16), 'tp', scatter_dimension=1, t...  20.5 us
    ppermute x3, starting transfers between devices, from_behind(): lax.ppermute(value, axis, [(source, source + steps) for source in range(f...  10.4 us
  transfers between devices with their start and end apart: 6, of which 3 were waited for; matrix products, arithmetic and copies ran while one was open for 0% of the time, Pallas kernels for 0%

commit v1 on v0

v1 whole, which is shorter than its diff:
```python
import functools

import jax
import jax.numpy as jnp
from jax import lax
from jax.experimental import pallas as pl
from jax.experimental.pallas import tpu as pltpu
from jax.sharding import PartitionSpec as P

MESH = pl.DeviceIdType.MESH
LAYERS = 3
HALO = 8
SEQS = 4
LOCAL = 32
SPAN = LOCAL + HALO
ROWS = SEQS * SPAN
D = 1024
BF = jnp.bfloat16
F32 = jnp.float32
SEMS = 192


def kernel(seq, gain, wv, wo, wi, taps, wout, out, IN, OUT, XG, HG, GX, CUR, NORM, lsem, ssem, rsem):
    sp = lax.axis_index("sp")
    z = lax.axis_index("tp")
    c = lax.rem(sp, 2)
    x = lax.rem(sp // 2, 4)
    y = sp // 8

    def dev(dx=0, dy=0, dz=0, dc=0):
        xx = lax.rem(x + dx + 4, 4)
        yy = lax.rem(y + dy + 4, 4)
        cc = lax.rem(c + dc, 2)
        return ((yy * 4 + xx) * 2 + cc, lax.rem(z + dz + 4, 4))

    succ = (lax.rem(sp + 1, 32), z)
    pred = (lax.rem(sp + 31, 32), z)
    partner = dev(dc=1)

    def at(i, step):
        return lax.rem(i + step + 4, 4)

    place = ((y, x), (x, y))
    local = []
    for col in range(2):
        i, j = place[col]
        for m, w in enumerate((wv, wo, wi)):
            local.append(
                pltpu.make_async_copy(
                    w.at[:, pl.ds(16 * col, 16), :], IN.at[:, c, col, i, j, m], lsem.at[len(local)]
                )
            )
            local[-1].start()
    xcopy = pltpu.make_async_copy(seq, XG.at[z], lsem.at[len(local)])
    xcopy.start()

    for layer in range(LAYERS):
        turned = jnp.transpose(wout[layer].astype(F32)).astype(BF)
        for col in range(2):
            i, j = place[col]
            OUT[layer, c, col, i, j, z] = turned[16 * col : 16 * col + 16]

    barrier = pltpu.get_barrier_semaphore()
    friends = [dev(dx=1), dev(dx=-1), dev(dx=2), dev(dy=1), dev(dy=-1), dev(dy=2)]
    friends += [dev(dz=1), dev(dz=-1), dev(dz=2), partner, succ, pred]
    for friend in friends:
        pl.semaphore_signal(barrier, inc=1, device_id=friend, device_id_type=MESH)
    pl.semaphore_wait(barrier, len(friends))

    sent = {}

    def send(key, src, dst, target):
        k = len(sent)
        copy = pltpu.make_async_remote_copy(
            src_ref=src,
            dst_ref=dst,
            send_sem=ssem.at[k],
            recv_sem=rsem.at[k],
            device_id=target,
            device_id_type=MESH,
        )
        copy.start()
        sent[key] = copy

    def share(key, ref, target):
        send(key, ref, ref, target)

    def arrived(key):
        sent[key].wait_recv()

    def peer(col, di, dj):
        return dev(dx=dj, dy=di) if col == 0 else dev(dx=di, dy=dj)

    BUF = {"i": IN, "o": OUT}

    def unit_first(unit):
        buf, layer = BUF[unit[0]], unit[1]
        for col in range(2):
            i, j = place[col]
            for step in (1, -1, 2):
                share((unit, col, "p1", step), buf.at[layer, c, col, i, j], peer(col, 0, step))

    def unit_a(unit):
        buf, layer = BUF[unit[0]], unit[1]
        for col in range(2):
            i, j = place[col]
            for step in (1, -1, 2):
                arrived((unit, col, "p1", step))
            row = buf.at[layer, c, col, i]
            for step in (1, -1):
                share((unit, col, "p2", step), row, peer(col, step, 0))
            share((unit, col, "d", 0), row, partner)

    def unit_b(unit):
        buf, layer = BUF[unit[0]], unit[1]
        for col in range(2):
            i, j = place[col]
            for step in (1, -1):
                arrived((unit, col, "p2", step))
                row = at(i, -step)
                half = pl.ds(0 if step == 1 else 2, 2)
                share((unit, col, "p3", step), buf.at[layer, c, col, row, half], peer(col, step, 0))
                share((unit, col, "d", step), buf.at[layer, c, col, row], partner)

    def unit_c(unit):
        buf, layer = BUF[unit[0]], unit[1]
        for col in range(2):
            i, j = place[col]
            row = at(i, 2)
            for step in (1, -1):
                arrived((unit, col, "p3", step))
            share((unit, col, "d", 2), buf.at[layer, c, col, row], partner)

    def unit_d(unit):
        for col in range(2):
            for step in (0, 1, -1, 2):
                arrived((unit, col, "d", step))

    for copy in local:
        copy.wait()
    unit_first(("i", 0))
    xcopy.wait()
    for step in (1, -1, 2):
        share(("x", step), XG.at[z], dev(dz=step))
    send("halo", XG.at[z, :, pl.ds(16, 16), :], HG.at[z], succ)
    for col in range(2):
        i, j = place[col]
        for step in (1, -1, 2):
            share(("wo", col, step), OUT.at[:, c, col, i, j, z], dev(dz=step))
    unit_first(("i", 1))
    unit_first(("i", 2))

    unit_a(("i", 0))
    arrived("halo")
    for step in (1, -1, 2):
        share(("h", step), HG.at[z], dev(dz=step))
    for col in range(2):
        for step in (1, -1, 2):
            arrived(("wo", col, step))
    unit_first(("o", 0))
    unit_a(("i", 1))
    unit_b(("i", 0))
    unit_first(("o", 1))
    unit_first(("o", 2))
    unit_a(("o", 0))
    unit_c(("i", 0))

    for step in (1, -1, 2):
        arrived(("x", step))
        arrived(("h", step))
    first = jnp.where(sp == 0, 0.0, 1.0).astype(F32)
    for s in range(SEQS):
        for zz in range(4):
            columns = pl.ds(256 * zz, 256)
            before = HG[zz, s].astype(F32)[16 - HALO :]
            CUR[pl.ds(SPAN * s, HALO), columns] = before * first
            CUR[pl.ds(SPAN * s + HALO, LOCAL), columns] = XG[zz, s].astype(F32)

    def normalise(layer):
        for r in range(0, ROWS, 32):
            wide = CUR[pl.ds(r, 32), :]
            scaled = wide * lax.rsqrt(jnp.mean(wide * wide, axis=-1, keepdims=True) + 1e-06)
            NORM[pl.ds(r, 32), :] = (scaled * gain[pl.ds(layer, 1), :]).astype(BF)

    def gate(layer):
        total = jnp.zeros((ROWS, 384), F32)
        for yy in range(4):
            tiles = []
            for xx in range(4):
                for cc in range(2):
                    for col in range(2):
                        i, j = (yy, xx) if col == 0 else (xx, yy)
                        tiles.append(
                            jnp.concatenate([IN[layer, cc, col, i, j, m] for m in range(3)], axis=1)
                        )
            weights = jnp.concatenate(tiles, axis=0)
            total = total + jnp.dot(
                NORM[:, pl.ds(256 * yy, 256)], weights, preferred_element_type=F32
            )
        total = total.astype(BF).astype(F32)
        value, outer, inner = total[:, :128], total[:, 128:256], total[:, 256:]
        product = inner * value
        filtered = taps[layer, pl.ds(0, 1), :] * pltpu.roll(product, 2, 0)
        filtered = filtered + taps[layer, pl.ds(1, 1), :] * pltpu.roll(product, 1, 0)
        filtered = filtered + taps[layer, pl.ds(2, 1), :] * product
        GX[layer, z] = (outer * filtered).astype(BF)
        for step in (1, -1, 2):
            share(("g", layer, step), GX.at[layer, z], dev(dz=step))

    def project(layer):
        for step in (1, -1, 2):
            arrived(("g", layer, step))
        gated = jnp.concatenate([GX[layer, zz] for zz in range(4)], axis=1)
        last = layer == LAYERS - 1

        def columns_of(yy):
            tiles = []
            for xx in range(4):
                for cc in range(2):
                    for col in range(2):
                        i, j = (yy, xx) if col == 0 else (xx, yy)
                        tiles.append(
                            jnp.concatenate([OUT[layer, cc, col, i, j, zz] for zz in range(4)], axis=1)
                        )
            weights = jnp.concatenate(tiles, axis=0)
            return lax.dot_general(
                gated, weights, (((1,), (1,)), ((), ())), preferred_element_type=F32
            )

        if last:
            total = columns_of(z)
            mine = pl.ds(pl.multiple_of(256 * z, 256), 256)
            total = CUR[:, mine] + total
            for s in range(SEQS):
                out[s] = total[SPAN * s + HALO : SPAN * (s + 1)].astype(BF)
        else:
            for yy in range(4):
                columns = pl.ds(256 * yy, 256)
                CUR[:, columns] = (CUR[:, columns] + columns_of(yy)).astype(BF).astype(F32)

    normalise(0)
    unit_d(("i", 0))
    gate(0)

    unit_b(("i", 1))
    unit_a(("i", 2))
    unit_b(("o", 0))
    unit_a(("o", 1))
    unit_c(("i", 1))
    unit_c(("o", 0))
    unit_d(("o", 0))
    project(0)
    normalise(1)
    unit_d(("i", 1))
    gate(1)

    unit_b(("o", 1))
    unit_a(("o", 2))
    unit_b(("i", 2))
    unit_c(("o", 1))
    unit_c(("i", 2))
    unit_d(("o", 1))
    project(1)
    normalise(2)
    unit_d(("i", 2))
    gate(2)

    unit_b(("o", 2))
    unit_c(("o", 2))
    unit_d(("o", 2))
    project(2)

    for copy in sent.values():
        copy.wait_send()


def body(sequence, norm_gain, weight_value, weight_outer, weight_inner, conv_taps, weight_out):
    anywhere = pl.BlockSpec(memory_space=pl.ANY)
    vmem = pl.BlockSpec(memory_space=pltpu.VMEM)
    return pl.pallas_call(
        kernel,
        out_shape=jax.ShapeDtypeStruct(sequence.shape, BF),
        in_specs=[anywhere, vmem, anywhere, anywhere, anywhere, vmem, vmem],
        out_specs=vmem,
        scratch_shapes=[
            pltpu.VMEM((LAYERS, 2, 2, 4, 4, 3, 16, 128), BF),
            pltpu.VMEM((LAYERS, 2, 2, 4, 4, 4, 16, 128), BF),
            pltpu.VMEM((4, SEQS, LOCAL, 256), BF),
            pltpu.VMEM((4, SEQS, 16, 256), BF),
            pltpu.VMEM((LAYERS, 4, ROWS, 128), BF),
            pltpu.VMEM((ROWS, D), F32),
            pltpu.VMEM((ROWS, D), BF),
            pltpu.SemaphoreType.DMA((8,)),
            pltpu.SemaphoreType.DMA((SEMS,)),
            pltpu.SemaphoreType.DMA((SEMS,)),
        ],
        compiler_params=pltpu.CompilerParams(collective_id=0, has_side_effects=True),
    )(sequence, norm_gain, weight_value, weight_outer, weight_inner, conv_taps, weight_out)


def solution(mesh):
    return jax.shard_map(
        body,
        mesh=mesh,
        in_specs=(
            P(None, "sp", "tp"),
            P(),
            P(None, "sp", "tp"),
            P(None, "sp", "tp"),
            P(None, "sp", "tp"),
            P(None, None, "tp"),
            P(None, "tp", "sp"),
        ),
        out_specs=P(None, "sp", "tp"),
        check_vma=False,
    )
```

time: 379 us -> 47.3 us (0.12)
  blocking collectives: 321 us -> 0 us
  Pallas kernels: 0 us -> 44.1 us
  waiting for transfers between devices: 21.6 us -> 0 us
  between operations: 13.4 us -> 0.01 us
  starting transfers between devices: 10.5 us -> 0 us
  matrix products: 4.77 us -> 0 us
  other arithmetic: 4.12 us -> 0 us
    all_gather x15 -> x0, blocking collectives: 321 us -> none  [the longest x9 217 us: folded(): lax.all_gather(part, axis, axis=dim, tiled=True)]
    pallas_call x0 -> x1, Pallas kernels: none -> 44.1 us  [body(): pl.pallas_call(kernel, out_shape=jax.ShapeDtypeStruct(sequence.shape, BF)...]
    reduce_scatter x3 -> x0, waiting for transfers between devices: 20.5 us -> none  [body(): lax.psum_scatter(terms.astype(jnp.bfloat16), 'tp', scatter_dimension=1, t...]
    ppermute x3 -> x0, starting transfers between devices: 10.4 us -> none  [from_behind(): lax.ppermute(value, axis, [(source, source + steps) for source in range(f...]
    dot_general x12 -> x0, matrix products: 4.77 us -> none  [the longest x3 2.8 us: project_columns(): return jnp.dot(gated_rows, weight_cols, preferred_element_type=jnp.float32)]
  transfers between devices with their start and end apart: 6 -> 0, of which waited for: 3 -> 0; matrix products, arithmetic and copies ran while one was open for 0% -> 0% of each run, Pallas kernels for 0% -> 0%
where the time goes in v1:
time: 47.3 us; the launch traced here: 47 us
  Pallas kernels  44.1 us (93%)
  local copies, waits for them, and re-layouts  2.94 us (6%)
    pallas_call x1, Pallas kernels, body(): pl.pallas_call(kernel, out_shape=jax.ShapeDtypeStruct(sequence.shape, BF)...  44.1 us
    unnamed x2, local copies, waits for them, and re-layouts  2.94 us

profile of v1, /device:TPU:1, one launch (start us, length us, event | category | flops | bytes accessed | tf_op | source)
XLA Modules:
  0.0 47.0 jit_solution(11013305993213979716)
XLA Ops:
  0.0 1.5 %copy.8.wout = bf16[3,128,32]{2,1,0:T(8,128)(2,1)} copy(bf16[3,128,32]{1,2,0:T(8,128)(2,1)} %param.13) | data formatting | bytes 49152 | tf_op args[6]
  1.5 44.1 %shard_map.73 = bf16[4,32,256]{2,1,0:T(8,128)(2,1)} custom-call(bf16[4,32,256]{2,1,0:T(8,128)(2,1)} %seq.1, f32[3,1024]{1,0:T(4,128)} %gain.1, bf16[3,32,128]{2,1,0:T(8,128)(2,1)} %wv.1, bf16[3,32,128]{2,1,0:T(8,128)(2,1)} %wo.1, bf16[3,32,128]{2,1,0:T(8,128)(2,1)} %wi.1, f32[3,3,128]{2,1,0:T(4,128)} %taps.1, bf16[3,128,32]{2,1,0:T(8,128)(2,1)} %copy.8.wout), custom_call_target="tpu_custom_call" | custom-call | tf_op jit(solution)/shard_map/pallas_call | solution.py:280
  45.6 1.5 %copy.10 = bf16[4,32,256]{2,1,0:T(8,128)(2,1)} copy(bf16[4,32,256]{2,1,0:T(8,128)(2,1)} %shard_map.73) | data formatting | bytes 131072

commit v2 on v1

--- a/solution.py
+++ b/solution.py
@@ -51,14 +51,17 @@
                 )
             )
             local[-1].start()
-    xcopy = pltpu.make_async_copy(seq, XG.at[z], lsem.at[len(local)])
+    weigh = []
+    for col in range(2):
+        i, j = place[col]
+        weigh.append(
+            pltpu.make_async_copy(
+                wout.at[:, pl.ds(16 * col, 16), :], OUT.at[:, c, col, i, j, z], lsem.at[len(local) + col]
+            )
+        )
+        weigh[-1].start()
+    xcopy = pltpu.make_async_copy(seq, XG.at[z], lsem.at[8])
     xcopy.start()
-
-    for layer in range(LAYERS):
-        turned = jnp.transpose(wout[layer].astype(F32)).astype(BF)
-        for col in range(2):
-            i, j = place[col]
-            OUT[layer, c, col, i, j, z] = turned[16 * col : 16 * col + 16]
 
     barrier = pltpu.get_barrier_semaphore()
     friends = [dev(dx=1), dev(dx=-1), dev(dx=2), dev(dy=1), dev(dy=-1), dev(dy=2)]
@@ -144,6 +147,7 @@
         share(("x", step), XG.at[z], dev(dz=step))
     send("halo", XG.at[z, :, pl.ds(16, 16), :], HG.at[z], succ)
     for col in range(2):
+        weigh[col].wait()
         i, j = place[col]
         for step in (1, -1, 2):
             share(("wo", col, step), OUT.at[:, c, col, i, j, z], dev(dz=step))
@@ -280,7 +284,7 @@
     return pl.pallas_call(
         kernel,
         out_shape=jax.ShapeDtypeStruct(sequence.shape, BF),
-        in_specs=[anywhere, vmem, anywhere, anywhere, anywhere, vmem, vmem],
+        in_specs=[anywhere, vmem, anywhere, anywhere, anywhere, vmem, anywhere],
         out_specs=vmem,
         scratch_shapes=[
             pltpu.VMEM((LAYERS, 2, 2, 4, 4, 3, 16, 128), BF),
@@ -290,12 +294,12 @@
             pltpu.VMEM((LAYERS, 4, ROWS, 128), BF),
             pltpu.VMEM((ROWS, D), F32),
             pltpu.VMEM((ROWS, D), BF),
-            pltpu.SemaphoreType.DMA((8,)),
+            pltpu.SemaphoreType.DMA((9,)),
             pltpu.SemaphoreType.DMA((SEMS,)),
             pltpu.SemaphoreType.DMA((SEMS,)),
         ],
         compiler_params=pltpu.CompilerParams(collective_id=0, has_side_effects=True),
-    )(sequence, norm_gain, weight_value, weight_outer, weight_inner, conv_taps, weight_out)
+    )(sequence, norm_gain, weight_value, weight_outer, weight_inner, conv_taps, jnp.swapaxes(weight_out, 1, 2))
 
 
 def solution(mesh):

time: 47.3 us -> 45.4 us (0.960)
  local copies, waits for them, and re-layouts: 2.94 us -> 1.47 us
    unnamed x2 -> x1, local copies, waits for them, and re-layouts: 2.94 us -> 1.47 us
where the time goes in v2:
time: 45.4 us; the launch traced here: 45.2 us
  Pallas kernels  43.7 us (96%)
  local copies, waits for them, and re-layouts  1.47 us (3%)
    pallas_call x1, Pallas kernels, body(): pl.pallas_call(kernel, out_shape=jax.ShapeDtypeStruct(sequence.shape, BF)...  43.7 us
    unnamed x1, local copies, waits for them, and re-layouts  1.47 us

profile of v2, /device:TPU:1, one launch (start us, length us, event | category | flops | bytes accessed | tf_op | source)
XLA Modules:
  0.0 45.2 jit_solution(15466082247816251525)
XLA Ops:
  0.0 43.7 %shard_map.73 = bf16[4,32,256]{2,1,0:T(8,128)(2,1)} custom-call(bf16[4,32,256]{2,1,0:T(8,128)(2,1)} %seq.1, f32[3,1024]{1,0:T(4,128)} %gain.1, bf16[3,32,128]{2,1,0:T(8,128)(2,1)} %wv.1, bf16[3,32,128]{2,1,0:T(8,128)(2,1)} %wo.1, bf16[3,32,128]{2,1,0:T(8,128)(2,1)} %wi.1, f32[3,3,128]{2,1,0:T(4,128)} %taps.1, bf16[3,32,128]{2,1,0:T(8,128)(2,1)} %bitcast.1), custom_call_target="tpu_custom_call" | custom-call | tf_op jit(solution)/shard_map/pallas_call | solution.py:284
  43.7 1.5 %copy.9 = bf16[4,32,256]{2,1,0:T(8,128)(2,1)} copy(bf16[4,32,256]{2,1,0:T(8,128)(2,1)} %shard_map.73) | data formatting | bytes 131072

commit v3 on v1

v3 whole, which is shorter than its diff:
```python
import functools

import jax
import jax.numpy as jnp
from jax import lax
from jax.experimental import pallas as pl
from jax.experimental.pallas import tpu as pltpu
from jax.sharding import PartitionSpec as P

MESH = pl.DeviceIdType.MESH
LAYERS = 3
HALO = 8
SEQS = 4
LOCAL = 32
SPAN = LOCAL + HALO
ROWS = SEQS * SPAN
D = 1024
BF = jnp.bfloat16
F32 = jnp.float32
SEMS = 48


def kernel(seq, gain, wv, wo, wi, taps, wout, out, IN, OUT, XG, HG, GX, CUR, NORM, GAIN, TAPS, sems):
    sp = lax.axis_index("sp")
    z = lax.axis_index("tp")
    c = lax.rem(sp, 2)
    x = lax.rem(sp // 2, 4)
    y = sp // 8

    def dev(dx=0, dy=0, dz=0, dc=0):
        xx = lax.rem(x + dx + 4, 4)
        yy = lax.rem(y + dy + 4, 4)
        cc = lax.rem(c + dc, 2)
        return ((yy * 4 + xx) * 2 + cc, lax.rem(z + dz + 4, 4))

    succ = (lax.rem(sp + 1, 32), z)
    pred = (lax.rem(sp + 31, 32), z)
    partner = dev(dc=1)
    place = ((y, x), (x, y))
    steps = (1, -1, 2)
    BUF = {"i": IN, "o": OUT}

    def at(i, step):
        return lax.rem(i + step + 4, 4)

    names = {}

    def sem(key):
        return sems.at[names.setdefault(key, len(names))]

    def fetch(key, src, dst):
        pltpu.make_async_copy(src, dst, sem(key)).start()

    def fetched(key, like):
        pltpu.make_async_copy(like, like, sem(key)).wait()

    def send(key, group, src, dst, target):
        pltpu.make_async_remote_copy(
            src_ref=src,
            dst_ref=dst,
            send_sem=sem(("sent", group)),
            recv_sem=sem(key),
            device_id=target,
            device_id_type=MESH,
        ).start()

    def share(key, group, ref, target):
        send(key, group, ref, ref, target)

    def waiter(key, group, like):
        return pltpu.make_async_remote_copy(
            src_ref=like,
            dst_ref=like,
            send_sem=sem(("sent", group)),
            recv_sem=sem(key),
            device_id=partner,
            device_id_type=MESH,
        )

    def arrived(key, group, like):
        waiter(key, group, like).wait_recv()

    def left(key, group, like):
        waiter(key, group, like).wait_send()

    def peer(col, di, dj):
        return dev(dx=dj, dy=di) if col == 0 else dev(dx=di, dy=dj)

    for col in range(2):
        i, j = place[col]
        for m, w in enumerate((wv, wo, wi)):
            fetch("li", w.at[:, pl.ds(16 * col, 16), :], IN.at[:, c, col, i, j, m])
    for col in range(2):
        i, j = place[col]
        fetch("lo", wout.at[:, pl.ds(16 * col, 16), :], OUT.at[:, c, col, i, j, z])
    fetch("lx", seq, XG.at[z])
    fetch("lg", gain, GAIN)
    fetch("lt", taps, TAPS)

    def barrier_step():
        barrier = pltpu.get_barrier_semaphore()
        friends = [dev(dx=1), dev(dx=-1), dev(dx=2), dev(dy=1), dev(dy=-1), dev(dy=2)]
        friends += [dev(dz=1), dev(dz=-1), dev(dz=2), partner, succ, pred]
        for friend in friends:
            pl.semaphore_signal(barrier, inc=1, device_id=friend, device_id_type=MESH)
        pl.semaphore_wait(barrier, len(friends))

    def head_first():
        fetched("li", IN.at[0, 0, 0, pl.ds(0, 2), pl.ds(0, 3)])
        for col in range(2):
            i, j = place[col]
            own = IN.at[0, c, col, i, j]
            for step in steps:
                share("head far" if step == 2 else "head near", "i1", own, peer(col, 0, step))
        for col in range(2):
            i, j = place[col]
            for step in steps:
                share("head early", "i2", IN.at[0, c, col, i, j], peer(col, step, 0))

    def head_near():
        arrived("head near", "i1", IN.at[0, 0, 0, 0])
        for col in range(2):
            i, j = place[col]
            for back in (1, -1):
                for step in steps:
                    share("head early", "i2", IN.at[0, c, col, i, at(j, back)], peer(col, step, 0))

    def head_far():
        arrived("head far", "i1", IN.at[0, 0, 0, 0, pl.ds(0, 2)])
        for col in range(2):
            i, j = place[col]
            for step in steps:
                share("head late", "i2", IN.at[0, c, col, i, at(j, 2)], peer(col, step, 0))
        for col in range(2):
            i, j = place[col]
            share("head twin", "id", IN.at[0, c, col, i], partner)

    def head_rest():
        arrived("head early", "i2", IN.at[0, :, 0, pl.ds(0, 3), pl.ds(0, 3)])
        arrived("head late", "i2", IN.at[0, :, 0, 0, pl.ds(0, 3)])
        for col in range(2):
            i, j = place[col]
            for step in steps:
                share("head twin", "id", IN.at[0, c, col, at(i, step)], partner)

    def head_done():
        arrived("head twin", "id", IN.at[0, 0])

    def first(kind, layer):
        buf = BUF[kind]
        for col in range(2):
            i, j = place[col]
            for step in steps:
                share((kind, layer, 1), kind + "1", buf.at[layer, c, col, i, j], peer(col, 0, step))

    def second(kind, layer):
        buf = BUF[kind]
        arrived((kind, layer, 1), kind + "1", buf.at[layer, :, 0, 0, pl.ds(0, 3)])
        for col in range(2):
            i, j = place[col]
            for step in steps:
                share((kind, layer, 2), kind + "2", buf.at[layer, c, col, i], peer(col, step, 0))

    def third(kind, layer):
        buf = BUF[kind]
        arrived((kind, layer, 2), kind + "2", buf.at[layer, :, 0, pl.ds(0, 3)])
        share((kind, layer, 3), kind + "d", buf.at[layer, c], partner)

    def done(kind, layer):
        arrived((kind, layer, 3), kind + "d", BUF[kind].at[layer, 0])

    def stage_w(layer):
        if layer == 0:
            fetched("lo", OUT.at[0, 0, 0, 0, pl.ds(0, 2), pl.ds(0, 3)])
        for col in range(2):
            i, j = place[col]
            for step in steps:
                share(("w", layer), "w", OUT.at[layer, c, col, i, j, z], dev(dz=step))

    def wait_w(layer):
        arrived(("w", layer), "w", OUT.at[0, 0, 0, 0, pl.ds(0, 2), pl.ds(0, 3)])

    def stage_x():
        fetched("lx", XG.at[0])
        send("halo", "halo", XG.at[z, :, pl.ds(16, 16), :], HG.at[z], succ)
        for step in steps:
            share("x", "x", XG.at[z], dev(dz=step))

    def stage_h():
        arrived("halo", "halo", HG.at[0])
        for step in steps:
            share("h", "h", HG.at[z], dev(dz=step))

    def wait_x():
        arrived("x", "x", XG.at[pl.ds(0, 3)])
        arrived("h", "h", HG.at[pl.ds(0, 3)])
        fetched("lg", GAIN)
        fetched("lt", TAPS)

    def gwait(layer):
        arrived(("g", layer), "g", GX.at[0, pl.ds(0, 3)])

    def finish():
        left("x", "x", XG.at[pl.ds(0, 3)])
        left("h", "h", HG.at[pl.ds(0, 3)])
        left("halo", "halo", HG.at[0])
        left(("g", 0), "g", GX.at[:, pl.ds(0, 3)])
        left(("w", 0), "w", OUT.at[:, 0, 0, 0, pl.ds(0, 2), pl.ds(0, 3)])
        for kind in "io":
            buf = BUF[kind]
            left((kind, 1, 1), kind + "1", buf.at[:, :, 0, 0, pl.ds(0, 3)])
            left((kind, 1, 2), kind + "2", buf.at[:, :, 0, pl.ds(0, 3)])
            left((kind, 1, 3), kind + "d", buf.at[:, 0])

    def assemble():
        begun = jnp.where(sp == 0, 0.0, 1.0).astype(F32)
        for s in range(SEQS):
            for zz in range(4):
                columns = pl.ds(256 * zz, 256)
                before = HG[zz, s].astype(F32)[16 - HALO :]
                CUR[pl.ds(SPAN * s, HALO), columns] = before * begun
                CUR[pl.ds(SPAN * s + HALO, LOCAL), columns] = XG[zz, s].astype(F32)

    def normalise(layer):
        for r in range(0, ROWS, 32):
            wide = CUR[pl.ds(r, 32), :]
            scaled = wide * lax.rsqrt(jnp.mean(wide * wide, axis=-1, keepdims=True) + 1e-06)
            NORM[pl.ds(r, 32), :] = (scaled * GAIN[pl.ds(layer, 1), :]).astype(BF)

    def gate(layer):
        total = jnp.zeros((ROWS, 384), F32)
        for yy in range(4):
            tiles = []
            for xx in range(4):
                for cc in range(2):
                    for col in range(2):
                        i, j = (yy, xx) if col == 0 else (xx, yy)
                        tiles.append(
                            jnp.concatenate([IN[layer, cc, col, i, j, m] for m in range(3)], axis=1)
                        )
            weights = jnp.concatenate(tiles, axis=0)
            total = total + jnp.dot(
                NORM[:, pl.ds(256 * yy, 256)], weights, preferred_element_type=F32
            )
        total = total.astype(BF).astype(F32)
        value, outer, inner = total[:, :128], total[:, 128:256], total[:, 256:]
        product = inner * value
        filtered = TAPS[layer, pl.ds(0, 1), :] * pltpu.roll(product, 2, 0)
        filtered = filtered + TAPS[layer, pl.ds(1, 1), :] * pltpu.roll(product, 1, 0)
        filtered = filtered + TAPS[layer, pl.ds(2, 1), :] * product
        GX[layer, z] = (outer * filtered).astype(BF)
        for step in (1, -1, 2):
            share(("g", layer), "g", GX.at[layer, z], dev(dz=step))

    def project(layer):
        gated = jnp.concatenate([GX[layer, zz] for zz in range(4)], axis=1)
        last = layer == LAYERS - 1

        def columns_of(yy):
            tiles = []
            for xx in range(4):
                for cc in range(2):
                    for col in range(2):
                        i, j = (yy, xx) if col == 0 else (xx, yy)
                        tiles.append(
                            jnp.concatenate([OUT[layer, cc, col, i, j, zz] for zz in range(4)], axis=1)
                        )
            weights = jnp.concatenate(tiles, axis=0)
            return lax.dot_general(
                gated, weights, (((1,), (1,)), ((), ())), preferred_element_type=F32
            )

        if last:
            total = columns_of(z)
            mine = pl.ds(pl.multiple_of(256 * z, 256), 256)
            total = CUR[:, mine] + total
            for s in range(SEQS):
                out[s] = total[SPAN * s + HALO : SPAN * (s + 1)].astype(BF)
        else:
            for yy in range(4):
                columns = pl.ds(256 * yy, 256)
                CUR[:, columns] = (CUR[:, columns] + columns_of(yy)).astype(BF).astype(F32)

    barrier_step()
    head_first()
    stage_w(0)
    stage_x()
    stage_w(1)
    stage_w(2)
    first("i", 1)
    first("i", 2)
    head_near()
    stage_h()
    head_far()
    wait_w(0)
    first("o", 0)
    second("i", 1)
    wait_w(1)
    first("o", 1)
    wait_w(2)
    first("o", 2)
    wait_x()
    assemble()
    normalise(0)
    head_rest()
    head_done()
    gate(0)
    second("o", 0)
    second("i", 2)
    third("i", 1)
    second("o", 1)
    third("o", 0)
    done("o", 0)
    gwait(0)
    project(0)
    normalise(1)
    done("i", 1)
    gate(1)
    second("o", 2)
    third("i", 2)
    third("o", 1)
    done("o", 1)
    gwait(1)
    project(1)
    normalise(2)
    done("i", 2)
    gate(2)
    third("o", 2)
    done("o", 2)
    gwait(2)
    project(2)
    finish()
    assert len(names) <= SEMS, len(names)


def body(sequence, norm_gain, weight_value, weight_outer, weight_inner, conv_taps, weight_out):
    anywhere = pl.BlockSpec(memory_space=pl.ANY)
    vmem = pl.BlockSpec(memory_space=pltpu.VMEM)
    return pl.pallas_call(
        kernel,
        out_shape=jax.ShapeDtypeStruct(sequence.shape, BF),
        in_specs=[anywhere] * 7,
        out_specs=vmem,
        scratch_shapes=[
            pltpu.VMEM((LAYERS, 2, 2, 4, 4, 3, 16, 128), BF),
            pltpu.VMEM((LAYERS, 2, 2, 4, 4, 4, 16, 128), BF),
            pltpu.VMEM((4, SEQS, LOCAL, 256), BF),
            pltpu.VMEM((4, SEQS, 16, 256), BF),
            pltpu.VMEM((LAYERS, 4, ROWS, 128), BF),
            pltpu.VMEM((ROWS, D), F32),
            pltpu.VMEM((ROWS, D), BF),
            pltpu.VMEM((LAYERS, D), F32),
            pltpu.VMEM((LAYERS, 3, 128), F32),
            pltpu.SemaphoreType.DMA((SEMS,)),
        ],
        compiler_params=pltpu.CompilerParams(collective_id=0, has_side_effects=True),
    )(sequence, norm_gain, weight_value, weight_outer, weight_inner, conv_taps, jnp.swapaxes(weight_out, 1, 2))


def solution(mesh):
    return jax.shard_map(
        body,
        mesh=mesh,
        in_specs=(
            P(None, "sp", "tp"),
            P(),
            P(None, "sp", "tp"),
            P(None, "sp", "tp"),
            P(None, "sp", "tp"),
            P(None, None, "tp"),
            P(None, "tp", "sp"),
        ),
        out_specs=P(None, "sp", "tp"),
        check_vma=False,
    )
```

time: 47.3 us -> 37.3 us (0.79)
  the two profiles are of different devices: /device:TPU:1 before, /device:TPU:0 now
where the time goes in v3:
time: 37.3 us; the launch traced here: 37.1 us
  Pallas kernels  35.6 us (95%)
  local copies, waits for them, and re-layouts  1.47 us (4%)
    pallas_call x1, Pallas kernels, body(): pl.pallas_call(kernel, out_shape=jax.ShapeDtypeStruct(sequence.shape, BF)...  35.6 us
    unnamed x1, local copies, waits for them, and re-layouts  1.47 us

profile of v3, /device:TPU:0, one launch (start us, length us, event | category | flops | bytes accessed | tf_op | source)
XLA Modules:
  0.0 37.1 jit_solution(6525041485506157705)
XLA Ops:
  0.0 35.6 %shard_map.73 = bf16[4,32,256]{2,1,0:T(8,128)(2,1)} custom-call(bf16[4,32,256]{2,1,0:T(8,128)(2,1)} %seq.1, f32[3,1024]{1,0:T(4,128)} %gain.1, bf16[3,32,128]{2,1,0:T(8,128)(2,1)} %wv.1, bf16[3,32,128]{2,1,0:T(8,128)(2,1)} %wo.1, bf16[3,32,128]{2,1,0:T(8,128)(2,1)} %wi.1, f32[3,3,128]{2,1,0:T(4,128)} %taps.1, bf16[3,32,128]{2,1,0:T(8,128)(2,1)} %bitcast.1), custom_call_target="tpu_custom_call" | custom-call | tf_op jit(solution)/shard_map/pallas_call | solution.py:339
  35.6 1.5 %copy.9 = bf16[4,32,256]{2,1,0:T(8,128)(2,1)} copy(bf16[4,32,256]{2,1,0:T(8,128)(2,1)} %shard_map.73) | data formatting | bytes 131072
